TPU v7x, 32 devices: a whole 2x2x4 slice. The times are simulated.
32 devices in a mesh: ep: 8 (over z, core), tp: 4 (over y, x).
Axes of the slice: x: 2, y: 2, z: 4, core: 2. Of those that a mesh axis runs over, the one named last changes fastest.
Arguments:
- tokens: bfloat16 [1024, 2048], P('ep'), may hold values from -6 to 6
- cotangent: bfloat16 [1024, 2048], P('ep'), may hold values from -6 to 6
- expert_ids: int32 [1024, 2], P('ep'), may hold values from 0 to 7, all different within a row; in each aligned block of 128 rows (0 to 127, 128 to 255, ...) at most 64 rows name the same one
- route_weight: bfloat16 [1024, 2], P('ep'), may hold values from 0.19921875 to 1
- gate_weight: bfloat16 [8, 1024, 2048], P('ep', 'tp'), may hold values from -0.125 to 0.125
- up_weight: bfloat16 [8, 1024, 2048], P('ep', 'tp'), may hold values from -0.125 to 0.125
- down_weight: bfloat16 [8, 1024, 2048], P('ep', 'tp'), may hold values from -0.1875 to 0.1875
Outputs:
- tokens_grad: bfloat16 [1024, 2048], P('ep', 'tp')
- route_weight_grad: float32 [1024, 2], P('ep')
- gate_weight_grad: float32 [8, 1024, 2048], P('ep', 'tp')
- up_weight_grad: float32 [8, 1024, 2048], P('ep', 'tp')
- down_weight_grad: float32 [8, 1024, 2048], P('ep', 'tp')
Inputs may be any that keep to these rules, and one draw needn't show every extreme that they name: `expert_ids`: within each aligned block of 128 rows every expert is named at most 64 times; the two experts of a row differ.
All inputs are finite; a program needn't handle non-finite values.
Results may differ from a plain program's by a relative error of at most 0.0058.
Values may be sent and summed in bfloat16 or wider, within the bound.
A program may use at most 64 MiB of HBM per device.

v0:
```python
import jax
import jax.numpy as jnp
from jax import lax
from jax.sharding import PartitionSpec as P


def per_device(tokens, cotangent, expert_ids, route_weight, gate_weight, up_weight, down_weight):
    tok_rows, model_width = tokens.shape
    top_count = expert_ids.shape[1]
    local_experts = gate_weight.shape[0]
    ep_size = lax.axis_size("ep")
    tp_size = lax.axis_size("tp")
    expert_count = local_experts * ep_size
    capacity = 2 * tok_rows * top_count // expert_count
    column_span = model_width // tp_size
    flat_ids = expert_ids.reshape(-1)
    routed = flat_ids.shape[0]
    member = (flat_ids[:, None] == jnp.arange(expert_count, dtype=jnp.int32)[None, :]).astype(
        jnp.int32
    )
    rank_slot = jnp.sum((jnp.cumsum(member, axis=0) - 1) * member, axis=1)
    slot_index = flat_ids * capacity + rank_slot
    buffer_rows = expert_count * capacity
    source_pair = (
        jnp.full((buffer_rows,), routed, jnp.int32)
        .at[slot_index]
        .set(jnp.arange(routed, dtype=jnp.int32))
    )
    filled = source_pair < routed
    safe_pair = jnp.minimum(source_pair, routed - 1)
    token_of = safe_pair // top_count
    zero_value = jnp.zeros((), tokens.dtype)
    send_weight = jnp.where(filled, route_weight.reshape(-1)[safe_pair], zero_value)
    offset = lax.axis_index("tp") * column_span
    token_cols = lax.dynamic_slice_in_dim(tokens, offset, column_span, 1)
    cotangent_cols = lax.dynamic_slice_in_dim(cotangent, offset, column_span, 1)
    part_tokens, part_cotangent, got_weight = (
        lax.all_to_all(token_cols[token_of], "ep", split_axis=0, concat_axis=0, tiled=True),
        lax.all_to_all(cotangent_cols[token_of], "ep", split_axis=0, concat_axis=0, tiled=True),
        lax.all_to_all(send_weight, "ep", split_axis=0, concat_axis=0, tiled=True),
    )
    got_tokens, got_cotangent = (
        lax.all_gather(part_tokens, "tp", axis=1, tiled=True),
        lax.all_gather(part_cotangent, "tp", axis=1, tiled=True),
    )
    block_shape = (ep_size, local_experts, capacity, model_width)
    routed_rows = got_tokens.reshape(block_shape)
    routed_cotangent = got_cotangent.reshape(block_shape)
    pair_weight = got_weight.reshape(ep_size, local_experts, capacity, 1).astype(jnp.float32)
    pre_gate = jnp.einsum(
        "secd,efd->secf", routed_rows, gate_weight, preferred_element_type=jnp.float32
    )
    pre_up = jnp.einsum(
        "secd,efd->secf", routed_rows, up_weight, preferred_element_type=jnp.float32
    )
    sigma = jax.nn.sigmoid(pre_gate)
    silu_gate = pre_gate * sigma
    hidden = silu_gate * pre_up
    back_hidden = jnp.einsum(
        "secd,efd->secf", routed_cotangent, down_weight, preferred_element_type=jnp.float32
    )
    pair_products = lax.psum(jnp.sum(hidden * back_hidden, axis=3), "tp")
    scaled = pair_weight * back_hidden
    grad_gate = (scaled * pre_up * sigma * (1.0 + pre_gate * (1.0 - sigma))).astype(jnp.bfloat16)
    grad_up = (scaled * silu_gate).astype(jnp.bfloat16)
    weighted = (pair_weight * hidden).astype(jnp.bfloat16)
    down_grad = jnp.einsum(
        "secf,secd->efd", weighted, routed_cotangent, preferred_element_type=jnp.float32
    )
    gate_grad = jnp.einsum(
        "secf,secd->efd", grad_gate, routed_rows, preferred_element_type=jnp.float32
    )
    up_grad = jnp.einsum("secf,secd->efd", grad_up, routed_rows, preferred_element_type=jnp.float32)
    full_gate, full_up = (
        lax.all_gather(grad_gate, "tp", axis=3, tiled=True),
        lax.all_gather(grad_up, "tp", axis=3, tiled=True),
    )
    gate_cols, up_cols = (
        lax.all_to_all(gate_weight, "tp", split_axis=2, concat_axis=1, tiled=True),
        lax.all_to_all(up_weight, "tp", split_axis=2, concat_axis=1, tiled=True),
    )
    pair_grad = (
        jnp.einsum("secf,efd->secd", full_gate, gate_cols, preferred_element_type=jnp.float32)
        + jnp.einsum("secf,efd->secd", full_up, up_cols, preferred_element_type=jnp.float32)
    ).astype(jnp.bfloat16)
    returned = lax.all_to_all(
        pair_grad.reshape(buffer_rows, column_span), "ep", split_axis=0, concat_axis=0, tiled=True
    )
    returned_products = lax.all_to_all(
        pair_products.reshape(buffer_rows), "ep", split_axis=0, concat_axis=0, tiled=True
    )
    per_pair = returned[slot_index].astype(jnp.float32).reshape(tok_rows, top_count, column_span)
    tokens_grad = jnp.sum(per_pair, axis=1).astype(jnp.bfloat16)
    route_grad = returned_products[slot_index].reshape(tok_rows, top_count)
    return (tokens_grad, route_grad, gate_grad, up_grad, down_grad)


def solution(mesh):
    in_specs = (
        P("ep", None),
        P("ep", None),
        P("ep", None),
        P("ep", None),
        P("ep", "tp", None),
        P("ep", "tp", None),
        P("ep", "tp", None),
    )
    out_specs = (
        P("ep", "tp"),
        P("ep", None),
        P("ep", "tp", None),
        P("ep", "tp", None),
        P("ep", "tp", None),
    )
    return jax.shard_map(
        per_device, mesh=mesh, in_specs=in_specs, out_specs=out_specs, check_vma=False
    )
```

profile of v0, /device:TPU:0, one launch (start us, length us, event | category | flops | bytes accessed | tf_op | source)
XLA Modules:
  0.0 231.4 jit_solution(7355271830630326382)
XLA Ops:
  14.7 21.6 %all_to_all.85 = bf16[8,64,512]{2,1,0:T(8,128)(2,1)} all-to-all(bf16[8,64,512]{2,1,0:T(8,128)(2,1)S(1)} %bitcast.112), channel_id=1, replica_groups=mesh['ep'=8,'tp'=4] {'ep'}, dimensions={0} | all-to-all | bytes 1048576 | tf_op jit(solution)/shard_map/all_to_all | solution.py:38
  38.4 18.5 %all_to_all.86 = bf16[8,64,512]{2,1,0:T(8,128)(2,1)} all-to-all(bf16[8,64,512]{2,1,0:T(8,128)(2,1)S(1)} %bitcast.111), channel_id=1, replica_groups=mesh['ep'=8,'tp'=4] {'ep'}, dimensions={0} | all-to-all | bytes 1048576 | tf_op jit(solution)/shard_map/all_to_all | solution.py:39
  57.3 3.4 %gather_fusion = bf16[512]{0:T(512)(128)(2,1)S(1)} fusion(bf16[256]{0:T(256)(128)(2,1)S(1)} %reshape.155, s32[1024]{0:T(1024)S(1)} %get-tuple-element.28), kind=kCustom, calls=%fused_computation | custom fusion | bytes 4096 | tf_op jit(solution)/shard_map/gather | solution.py:33
  60.8 8.1 %all_to_all.87 = bf16[8,64,1]{1,2,0:T(2,128)(2,1)S(1)} all-to-all(bf16[8,64,1]{1,2,0:T(2,128)(2,1)S(1)} %all_to_all.77), channel_id=1, replica_groups=mesh['ep'=8,'tp'=4] {'ep'}, dimensions={0} | all-to-all | bytes 2048 | tf_op jit(solution)/shard_map/all_to_all | solution.py:40
  70.5 3.3 %convolution_bitcast_fusion.4 = f32[8,1,64,256]{3,2,0,1:T(8,128)} fusion(bf16[8,64,2048]{2,1,0:T(8,128)(2,1)} %bitcast.101, bf16[1,256,2048]{2,1,0:T(8,128)(2,1)S(1)} %copy-done.5), kind=kOutput, calls=%fused_computation.12 | convolution fusion | flops 536870912 | bytes 3670016 | tf_op jit(solution)/shard_map/secd,efd->secf/dot_general | solution.py:53
  74.5 32.8 %all-gather.5.cloned.1.call-done = bf16[512,2048]{1,0:T(8,128)(2,1)} async-done(((bf16[512,512]{1,0:T(8,128)(2,1)}), bf16[512,2048]{1,0:T(8,128)(2,1)}) %all-gather.5.cloned.1.call-update) | async-done | bytes 2097168 | tf_op jit(solution)/shard_map/all_gather | solution.py:44
  107.4 3.3 %multiply_reduce_fusion = (f32[8,64]{1,0:T(8,128)S(1)}, bf16[8,1,64,256]{3,2,0,1:T(8,128)(2,1)}, bf16[8,1,64,256]{3,2,0,1:T(8,128)(2,1)}) fusion(f32[8,1,64,256]{3,2,0,1:T(8,128)S(1)} %copy-done.9, f32[8,1,64,256]{3,2,0,1:T(8,128)S(1)} %convolution_bitcast_fusion.3, f32[8,64]{1,0:T(8,128)S(1)} %bitcast.117, bf16[8,64,2048]{2,1,0:T(8,128)(2,1)} %bitcast.109, ...), kind=kOutput, calls=%fused_computation.21 | convolution fusion | flops 539098624 | bytes 4722688 | tf_op jit(solution)/shard_map/secd,efd->secf/dot_general | solution.py:59
  110.6 4.6 %copy.35 = bf16[1,256,2048]{1,0,2:T(2,128)(2,1)S(1)} copy(bf16[1,256,2048]{2,1,0:T(8,128)(2,1)} %param.11) | data formatting | bytes 2097152 | tf_op args[4]
  115.8 11.6 %reduce.8 = bf16[2048,256]{1,0:T(8,128)(2,1)} reduce(bf16[2048,1,256]{2,1,0:T(2,128)(2,1)S(1)} %bitcast.105, bf16[]{:T(256)} %broadcast.123), dimensions={1}, to_apply=%bitcast.84.reduce_sub_computation | reduce | bytes 2097154
  127.3 3.5 %reshape.242 = bf16[4,2,65536]{2,1,0:T(2,128)(2,1)} reshape(bf16[2048,256]{1,0:T(8,128)(2,1)} %reduce.8) | data formatting | bytes 2097152
  130.8 4.2 %all-to-all-start.3 = ((bf16[4,2,65536]{2,1,0:T(2,128)(2,1)}), bf16[4,2,65536]{2,1,0:T(2,128)(2,1)}, u32[]{:S(2)}, u32[]{:S(2)}) async-start(bf16[4,2,65536]{2,1,0:T(2,128)(2,1)} %reshape.242), calls=%async_computation.3 | async-start | bytes 2097152 | tf_op jit(solution)/shard_map/all_to_all | solution.py:79
  135.6 4.6 %copy.37 = bf16[1,256,2048]{1,0,2:T(2,128)(2,1)S(1)} copy(bf16[1,256,2048]{2,1,0:T(8,128)(2,1)} %param.12) | data formatting | bytes 2097152 | tf_op args[5]
  140.3 11.6 %reduce.9 = bf16[2048,256]{1,0:T(8,128)(2,1)} reduce(bf16[2048,1,256]{2,1,0:T(2,128)(2,1)S(1)} %bitcast.106, bf16[]{:T(256)} %broadcast.123), dimensions={1}, to_apply=%bitcast.86.reduce_sub_computation | reduce | bytes 2097154
  151.8 3.5 %reshape.244 = bf16[4,2,65536]{2,1,0:T(2,128)(2,1)} reshape(bf16[2048,256]{1,0:T(8,128)(2,1)} %reduce.9) | data formatting | bytes 2097152
  155.3 4.3 %all-to-all-start.4 = ((bf16[4,2,65536]{2,1,0:T(2,128)(2,1)}), bf16[4,2,65536]{2,1,0:T(2,128)(2,1)}, u32[]{:S(2)}, u32[]{:S(2)}) async-start(bf16[4,2,65536]{2,1,0:T(2,128)(2,1)} %reshape.244), calls=%async_computation.4 | async-start | bytes 2097152 | tf_op jit(solution)/shard_map/all_to_all | solution.py:80
  159.6 2.6 %reshape.243 = bf16[2048,1,256]{2,1,0:T(2,128)(2,1)S(1)} reshape(bf16[4,2,65536]{2,1,0:T(2,128)(2,1)} %all-to-all-done.3) | data formatting | bytes 2097152
  165.6 10.7 %all-to-all-done.4 = bf16[4,2,65536]{2,1,0:T(2,128)(2,1)} async-done(((bf16[4,2,65536]{2,1,0:T(2,128)(2,1)}), bf16[4,2,65536]{2,1,0:T(2,128)(2,1)}, u32[]{:S(2)}, u32[]{:S(2)}) %all-to-all-start.4) | async-done | bytes 1048608 | tf_op jit(solution)/shard_map/all_to_all | solution.py:80
  181.7 9.5 %psum.7 = f32[8,64,1]{1,2,0:T(1,128)} all-reduce(f32[8,64,1]{1,2,0:T(1,128)S(1)} %bitcast.121), channel_id=1, replica_groups=mesh['ep'=8,'tp'=4] {'tp'}, use_global_device_ids=true, to_apply=%region_6.7 | all-reduce | flops 512 | bytes 4096 | tf_op jit(solution)/shard_map/psum | solution.py:62
  191.3 4.6 %all-to-all-start.6 = ((f32[8,64,1]{1,2,0:T(1,128)}), f32[8,64,1]{1,2,0:T(1,128)S(1)}, u32[]{:S(2)}, u32[]{:S(2)}) async-start(f32[8,64,1]{1,2,0:T(1,128)} %psum.7), calls=%async_computation.6 | async-start | bytes 8192 | tf_op jit(solution)/shard_map/all_to_all | solution.py:89
  195.9 2.9 %fusion.2 = f32[8,64,512]{2,1,0:T(8,128)} fusion(bf16[1024,512,1]{1,0,2:T(8,128)(2,1)S(1)} %bitcast.115, bf16[8,1,64,1024]{3,2,0,1:T(8,128)(2,1)} %all-gather.9.cloned.1.call-done), kind=kOutput, calls=%fused_computation.15 | convolution fusion | flops 536870912 | bytes 3145728 | tf_op jit(solution)/shard_map/secf,efd->secd/dot_general | solution.py:83
  198.8 3.1 %fusion = bf16[8,64,512]{2,1,0:T(8,128)(2,1)} fusion(f32[8,64,512]{2,1,0:T(8,128)} %fusion.2, bf16[1024,512,1]{1,0,2:T(8,128)(2,1)S(1)} %bitcast.116, bf16[8,1,64,1024]{3,2,0,1:T(8,128)(2,1)} %all-gather.11.cloned.1.call-done), kind=kOutput, calls=%fused_computation.10 | convolution fusion | flops 537395200 | bytes 3670016 | tf_op jit(solution)/shard_map/secf,efd->secd/dot_general | solution.py:84
  201.9 5.1 %all-to-all-start.5 = ((bf16[8,64,512]{2,1,0:T(8,128)(2,1)}), bf16[8,64,512]{2,1,0:T(8,128)(2,1)S(1)}, u32[]{:S(2)}, u32[]{:S(2)}) async-start(bf16[8,64,512]{2,1,0:T(8,128)(2,1)} %fusion), calls=%async_computation.5 | async-start | bytes 1048576 | tf_op jit(solution)/shard_map/all_to_all | solution.py:86
  207.0 3.8 %convolution_bitcast_fusion.2 = f32[1,256,2048]{2,1,0:T(8,128)} fusion(bf16[8,64,2048]{2,1,0:T(8,128)(2,1)} %bitcast.102, bf16[8,1,64,256]{3,2,0,1:T(8,128)(2,1)S(1)} %copy-done.7), kind=kOutput, calls=%fused_computation.8 | convolution fusion | flops 536870912 | bytes 4456448 | tf_op jit(solution)/shard_map/secf,secd->efd/dot_general | solution.py:70
  219.2 3.1 %all-to-all-done.5 = bf16[8,64,512]{2,1,0:T(8,128)(2,1)S(1)} async-done(((bf16[8,64,512]{2,1,0:T(8,128)(2,1)}), bf16[8,64,512]{2,1,0:T(8,128)(2,1)S(1)}, u32[]{:S(2)}, u32[]{:S(2)}) %all-to-all-start.5) | async-done | bytes 524320 | tf_op jit(solution)/shard_map/all_to_all | solution.py:86
  (85 shorter events, 33.2 us)
Async XLA Ops:
  7.2 100.2 %copy-start = (bf16[1,256,2048]{2,1,0:T(8,128)(2,1)S(1)}, bf16[1,256,2048]{2,1,0:T(8,128)(2,1)}, u32[]{:S(2)}) copy-start(bf16[1,256,2048]{2,1,0:T(8,128)(2,1)} %param.13) | copy-start | bytes 3145732
  7.2 63.3 %all-gather.7.cloned.1.call-start = ((), (), s32[]{:S(2)}) async-start(), calls=%async_computation.8 | async-start | bytes 2621440 | tf_op jit(solution)/shard_map/all_gather | solution.py:43
  36.3 71.0 %all-gather.5.cloned.1.call-start = ((), (), s32[]{:S(2)}) async-start(), calls=%async_computation.7 | async-start | bytes 2621440 | tf_op jit(solution)/shard_map/all_gather | solution.py:44
  36.4 20.6 %copy-start.13 = (bf16[128,2]{0,1:T(2,128)(2,1)S(1)}, bf16[128,2]{0,1:T(2,128)(2,1)}, u32[]{:S(2)}) copy-start(bf16[128,2]{0,1:T(2,128)(2,1)} %param.10) | copy-start | bytes 1540
  38.4 32.1 %copy-start.5 = (bf16[1,256,2048]{2,1,0:T(8,128)(2,1)S(1)}, bf16[1,256,2048]{2,1,0:T(8,128)(2,1)}, u32[]{:S(2)}) copy-start(bf16[1,256,2048]{2,1,0:T(8,128)(2,1)} %param.12) | copy-start | bytes 3145732
  56.9 138.9 %all-gather.9.cloned.1.call-start = ((), (), s32[]{:S(2)}) async-start(), calls=%async_computation.9 | async-start | bytes 1310720 | tf_op jit(solution)/shard_map/all_gather | solution.py:75
  60.7 13.1 %copy-start.4 = (bf16[1,256,2048]{2,1,0:T(8,128)(2,1)S(1)}, bf16[1,256,2048]{2,1,0:T(8,128)(2,1)}, u32[]{:S(2)}) copy-start(bf16[1,256,2048]{2,1,0:T(8,128)(2,1)} %param.11) | copy-start | bytes 3145732
  70.5 3.3 %copy-start.1 = (bf16[512,2048]{1,0:T(8,128)(2,1)S(1)}, bf16[512,2048]{1,0:T(8,128)(2,1)}, u32[]{:S(2)}) copy-start(bf16[512,2048]{1,0:T(8,128)(2,1)} %all-gather.7.cloned.1.call-done) | copy-start | bytes 6291460
  73.8 33.6 %copy-start.9 = (f32[8,1,64,256]{3,2,0,1:T(8,128)S(1)}, f32[8,1,64,256]{3,2,0,1:T(8,128)}, u32[]{:S(2)}) copy-start(f32[8,1,64,256]{3,2,0,1:T(8,128)} %convolution_bitcast_fusion.4) | copy-start | bytes 1572868
  74.5 36.1 %copy-start.11 = (f32[8,1,64,256]{3,2,0,1:T(8,128)}, f32[8,1,64,256]{3,2,0,1:T(8,128)S(1)}, u32[]{:S(2)}) copy-start(f32[8,1,64,256]{3,2,0,1:T(8,128)S(1)} %convolution_bitcast_fusion.3) | copy-start | bytes 1572868
  130.8 24.5 %all-to-all-start.3 = ((bf16[4,2,65536]{2,1,0:T(2,128)(2,1)}), bf16[4,2,65536]{2,1,0:T(2,128)(2,1)}, u32[]{:S(2)}, u32[]{:S(2)}) async-start(bf16[4,2,65536]{2,1,0:T(2,128)(2,1)} %reshape.242), calls=%async_computation.3 | async-start | bytes 2097152 | tf_op jit(solution)/shard_map/all_to_all | solution.py:79
  135.1 63.7 %all-gather.11.cloned.1.call-start = ((), (), s32[]{:S(2)}) async-start(), calls=%async_computation.10 | async-start | bytes 1310720 | tf_op jit(solution)/shard_map/all_gather | solution.py:76
  155.3 21.1 %all-to-all-start.4 = ((bf16[4,2,65536]{2,1,0:T(2,128)(2,1)}), bf16[4,2,65536]{2,1,0:T(2,128)(2,1)}, u32[]{:S(2)}, u32[]{:S(2)}) async-start(bf16[4,2,65536]{2,1,0:T(2,128)(2,1)} %reshape.244), calls=%async_computation.4 | async-start | bytes 2097152 | tf_op jit(solution)/shard_map/all_to_all | solution.py:80
  180.1 15.7 %copy-start.8 = (bf16[1,4,256,512]{3,2,1,0:T(8,128)(2,1)S(1)}, bf16[1,4,256,512]{3,2,1,0:T(8,128)(2,1)}, u32[]{:S(2)}) copy-start(bf16[1,4,256,512]{3,2,1,0:T(8,128)(2,1)} %copy.36) | copy-start | bytes 3145732
  191.3 10.6 %all-to-all-start.6 = ((f32[8,64,1]{1,2,0:T(1,128)}), f32[8,64,1]{1,2,0:T(1,128)S(1)}, u32[]{:S(2)}, u32[]{:S(2)}) async-start(f32[8,64,1]{1,2,0:T(1,128)} %psum.7), calls=%async_computation.6 | async-start | bytes 8192 | tf_op jit(solution)/shard_map/all_to_all | solution.py:89
  198.8 8.2 %copy-start.7 = (bf16[8,1,64,256]{3,2,0,1:T(8,128)(2,1)S(1)}, bf16[8,1,64,256]{3,2,0,1:T(8,128)(2,1)}, u32[]{:S(2)}) copy-start(bf16[8,1,64,256]{3,2,0,1:T(8,128)(2,1)} %get-tuple-element.21) | copy-start | bytes 786436
  201.9 20.4 %all-to-all-start.5 = ((bf16[8,64,512]{2,1,0:T(8,128)(2,1)}), bf16[8,64,512]{2,1,0:T(8,128)(2,1)S(1)}, u32[]{:S(2)}, u32[]{:S(2)}) async-start(bf16[8,64,512]{2,1,0:T(8,128)(2,1)} %fusion), calls=%async_computation.5 | async-start | bytes 1048576 | tf_op jit(solution)/shard_map/all_to_all | solution.py:86
  207.0 3.8 %copy-start.2 = (bf16[512,2048]{1,0:T(8,128)(2,1)S(1)}, bf16[512,2048]{1,0:T(8,128)(2,1)}, u32[]{:S(2)}) copy-start(bf16[512,2048]{1,0:T(8,128)(2,1)} %all-gather.7.cloned.1.call-done) | copy-start | bytes 6291460
  207.0 3.8 %copy-start.6 = (bf16[8,1,64,256]{3,2,0,1:T(8,128)(2,1)S(1)}, bf16[8,1,64,256]{3,2,0,1:T(8,128)(2,1)}, u32[]{:S(2)}) copy-start(bf16[8,1,64,256]{3,2,0,1:T(8,128)(2,1)} %get-tuple-element.22) | copy-start | bytes 786436
  210.8 2.1 copy-start.3
  210.8 2.1 copy-start.10
  210.8 2.3 copy-start.12
Sparse Core Ops, SparseCore 0:
  36.4 33.9 all-gather.6
  72.3 35.0 all-gather.4
  110.8 26.3 all-gather.8
  138.8 34.8 all-gather.10
where the time goes:
time: 233 us; the launch traced here: 231 us
  blocking collectives  57.7 us (25%)
  waiting for transfers between devices  48.6 us (21%)
  local copies, waits for them, and re-layouts  44.5 us (19%)
  other arithmetic  26.7 us (11%)
  matrix products  21.3 us (9%)
  starting transfers between devices  18.5 us (8%)
  between operations  14.1 us (6%)
    all_gather x1, waiting for transfers between devices, per_device(): lax.all_gather(part_cotangent, 'tp', axis=1, tiled=True)  32.8 us
    unnamed x40, local copies, waits for them, and re-layouts  26 us
    unnamed x2, other arithmetic  23.1 us
    all_to_all x1, blocking collectives, per_device(): lax.all_to_all(token_cols[token_of], 'ep', split_axis=0, concat_axis=0, t...  21.6 us
    all_to_all x1, blocking collectives, per_device(): lax.all_to_all(cotangent_cols[token_of], 'ep', split_axis=0, concat_axis=...  18.5 us
    all_to_all x1, waiting for transfers between devices, per_device(): lax.all_to_all(up_weight, 'tp', split_axis=2, concat_axis=1, tiled=True)  10.7 us
    psum x1, blocking collectives, per_device(): pair_products = lax.psum(jnp.sum(hidden * back_hidden, axis=3), 'tp')  9.53 us
    all_to_all x1, blocking collectives, per_device(): lax.all_to_all(send_weight, 'ep', split_axis=0, concat_axis=0, tiled=True)  8.07 us
  transfers between devices with their start and end apart: 8, of which 4 were waited for; matrix products, arithmetic and copies ran while one was open for 34% of the time, Pallas kernels for 0%

commit v1 on v0

--- a/solution.py
+++ b/solution.py
@@ -2,6 +2,13 @@
 import jax.numpy as jnp
 from jax import lax
 from jax.sharding import PartitionSpec as P
+
+
+def trade_parts(x, axis, split, join):
+    size = lax.axis_size(axis)
+    blocks = jnp.stack(jnp.split(x, size, axis=split), axis=0)
+    blocks = lax.all_to_all(blocks, axis, split_axis=0, concat_axis=0)
+    return jnp.concatenate(blocks, axis=join)
 
 
 def per_device(tokens, cotangent, expert_ids, route_weight, gate_weight, up_weight, down_weight):
@@ -77,7 +84,7 @@
     )
     gate_cols, up_cols = (
         lax.all_to_all(gate_weight, "tp", split_axis=2, concat_axis=1, tiled=True),
-        lax.all_to_all(up_weight, "tp", split_axis=2, concat_axis=1, tiled=True),
+        trade_parts(up_weight, "tp", 2, 1),
     )
     pair_grad = (
         jnp.einsum("secf,efd->secd", full_gate, gate_cols, preferred_element_type=jnp.float32)

time: 233 us -> 216 us (0.927)
  local copies, waits for them, and re-layouts: 44.5 us -> 30.5 us
  other arithmetic: 26.7 us -> 16.2 us
  blocking collectives: 57.7 us -> 65.4 us
  waiting for transfers between devices: 48.6 us -> 52.4 us
  starting transfers between devices: 18.5 us -> 16 us
    all_to_all x1, waiting for transfers between devices: 0.01 us -> 12 us  [per_device(): lax.all_to_all(gate_weight, 'tp', split_axis=2, concat_axis=1, tiled=True)]
    unnamed x40 -> x38, local copies, waits for them, and re-layouts: 26 us -> 14.3 us
    unnamed x2 -> x1, other arithmetic: 23.1 us -> 11.6 us
    all_to_all x1, waiting for transfers between devices: 10.7 us -> 0.01 us  [trade_parts(): blocks = lax.all_to_all(blocks, axis, split_axis=0, concat_axis=0)]
    psum x1, blocking collectives: 9.53 us -> 17.2 us  [per_device(): pair_products = lax.psum(jnp.sum(hidden * back_hidden, axis=3), 'tp')]
    all_to_all x1, waiting for transfers between devices: 0.01 us -> 2.37 us  [per_device(): lax.all_to_all(pair_products.reshape(buffer_rows), 'ep', split_axis=0, co...]
  transfers between devices with their start and end apart: 8 -> 8, of which waited for: 4 -> 5; matrix products, arithmetic and copies ran while one was open for 34% -> 25% of each run, Pallas kernels for 0% -> 0%
where the time goes in v1:
time: 216 us; the launch traced here: 215 us
  blocking collectives  65.4 us (30%)
  waiting for transfers between devices  52.4 us (24%)
  local copies, waits for them, and re-layouts  30.5 us (14%)
  matrix products  20.4 us (9%)
  other arithmetic  16.2 us (8%)
  starting transfers between devices  16 us (7%)
  between operations  14.1 us (7%)
    all_gather x1, waiting for transfers between devices, per_device(): lax.all_gather(part_cotangent, 'tp', axis=1, tiled=True)  32.8 us
    all_to_all x1, blocking collectives, per_device(): lax.all_to_all(token_cols[token_of], 'ep', split_axis=0, concat_axis=0, t...  21.6 us
    all_to_all x1, blocking collectives, per_device(): lax.all_to_all(cotangent_cols[token_of], 'ep', split_axis=0, concat_axis=...  18.5 us
    psum x1, blocking collectives, per_device(): pair_products = lax.psum(jnp.sum(hidden * back_hidden, axis=3), 'tp')  17.2 us
    unnamed x38, local copies, waits for them, and re-layouts  14.3 us
    all_to_all x1, waiting for transfers between devices, per_device(): lax.all_to_all(gate_weight, 'tp', split_axis=2, concat_axis=1, tiled=True)  12 us
    unnamed x1, other arithmetic  11.6 us
    all_to_all x1, blocking collectives, per_device(): lax.all_to_all(send_weight, 'ep', split_axis=0, concat_axis=0, tiled=True)  8.07 us
  transfers between devices with their start and end apart: 8, of which 5 were waited for; matrix products, arithmetic and copies ran while one was open for 25% of the time, Pallas kernels for 0%

profile of v1, /device:TPU:0, one launch (start us, length us, event | category | flops | bytes accessed | tf_op | source)
XLA Modules:
  0.0 214.9 jit_solution(410958308754793971)
XLA Ops:
  12.7 2.0 gather_fusion.2
  14.7 21.6 %all_to_all.78 = bf16[8,64,512]{2,1,0:T(8,128)(2,1)} all-to-all(bf16[8,64,512]{2,1,0:T(8,128)(2,1)S(1)} %bitcast.120), channel_id=1, replica_groups=mesh['ep'=8,'tp'=4] {'ep'}, dimensions={0} | all-to-all | bytes 1048576 | tf_op jit(solution)/shard_map/all_to_all | solution.py:45
  38.4 18.5 %all_to_all.79 = bf16[8,64,512]{2,1,0:T(8,128)(2,1)} all-to-all(bf16[8,64,512]{2,1,0:T(8,128)(2,1)S(1)} %bitcast.119), channel_id=1, replica_groups=mesh['ep'=8,'tp'=4] {'ep'}, dimensions={0} | all-to-all | bytes 1048576 | tf_op jit(solution)/shard_map/all_to_all | solution.py:46
  57.3 3.4 %gather_fusion = bf16[512]{0:T(512)(128)(2,1)S(1)} fusion(bf16[256]{0:T(256)(128)(2,1)S(1)} %reshape.158, s32[1024]{0:T(1024)S(1)} %get-tuple-element.32), kind=kCustom, calls=%fused_computation | custom fusion | bytes 4096 | tf_op jit(solution)/shard_map/gather | solution.py:40
  60.8 8.1 %all_to_all.80 = bf16[8,64,1]{1,2,0:T(2,128)(2,1)S(1)} all-to-all(bf16[8,64,1]{1,2,0:T(2,128)(2,1)S(1)} %all_to_all.70), channel_id=1, replica_groups=mesh['ep'=8,'tp'=4] {'ep'}, dimensions={0} | all-to-all | bytes 2048 | tf_op jit(solution)/shard_map/all_to_all | solution.py:47
  70.5 3.3 %convolution_bitcast_fusion.5 = f32[8,1,64,256]{3,2,0,1:T(8,128)} fusion(bf16[8,64,2048]{2,1,0:T(8,128)(2,1)} %bitcast.111, bf16[1,256,2048]{2,1,0:T(8,128)(2,1)S(1)} %copy-done.8), kind=kOutput, calls=%fused_computation.14 | convolution fusion | flops 536870912 | bytes 3670016 | tf_op jit(solution)/shard_map/secd,efd->secf/dot_general | solution.py:60
  74.5 32.8 %all-gather.5.cloned.1.call-done = bf16[512,2048]{1,0:T(8,128)(2,1)} async-done(((bf16[512,512]{1,0:T(8,128)(2,1)}), bf16[512,2048]{1,0:T(8,128)(2,1)}) %all-gather.5.cloned.1.call-update) | async-done | bytes 2097168 | tf_op jit(solution)/shard_map/all_gather | solution.py:51
  107.4 3.3 %multiply_reduce_fusion = (f32[8,64]{1,0:T(8,128)S(1)}, bf16[8,1,64,256]{3,2,0,1:T(8,128)(2,1)}, bf16[8,1,64,256]{3,2,0,1:T(8,128)(2,1)}) fusion(f32[8,1,64,256]{3,2,0,1:T(8,128)S(1)} %copy-done.10, f32[8,1,64,256]{3,2,0,1:T(8,128)S(1)} %convolution_bitcast_fusion.4, f32[8,64]{1,0:T(8,128)S(1)} %bitcast.124, bf16[8,64,2048]{2,1,0:T(8,128)(2,1)} %bitcast.117, ...), kind=kOutput, calls=%fused_computation.23 | convolution fusion | flops 539098624 | bytes 4722688 | tf_op jit(solution)/shard_map/secd,efd->secf/dot_general | solution.py:66
  110.7 4.6 %copy.31 = bf16[1,256,2048]{1,0,2:T(2,128)(2,1)S(1)} copy(bf16[1,256,2048]{2,1,0:T(8,128)(2,1)} %param.11) | data formatting | bytes 2097152 | tf_op args[4]
  115.8 11.6 %reduce.8 = bf16[2048,256]{1,0:T(8,128)(2,1)} reduce(bf16[2048,1,256]{2,1,0:T(2,128)(2,1)S(1)} %bitcast.115, bf16[]{:T(256)} %broadcast.123), dimensions={1}, to_apply=%bitcast.97.reduce_sub_computation | reduce | bytes 2097154
  127.4 3.6 %reshape.245 = bf16[4,2,65536]{2,1,0:T(2,128)(2,1)} reshape(bf16[2048,256]{1,0:T(8,128)(2,1)} %reduce.8) | data formatting | bytes 2097152
  130.9 3.5 %all-to-all-start.3 = ((bf16[4,2,65536]{2,1,0:T(2,128)(2,1)}), bf16[4,2,65536]{2,1,0:T(2,128)(2,1)S(1)}, u32[]{:S(2)}, u32[]{:S(2)}) async-start(bf16[4,2,65536]{2,1,0:T(2,128)(2,1)} %reshape.245), calls=%async_computation.3 | async-start | bytes 2097152 | tf_op jit(solution)/shard_map/all_to_all | solution.py:86
  136.3 12.0 %all-to-all-done.3 = bf16[4,2,65536]{2,1,0:T(2,128)(2,1)S(1)} async-done(((bf16[4,2,65536]{2,1,0:T(2,128)(2,1)}), bf16[4,2,65536]{2,1,0:T(2,128)(2,1)S(1)}, u32[]{:S(2)}, u32[]{:S(2)}) %all-to-all-start.3) | async-done | bytes 1048608 | tf_op jit(solution)/shard_map/all_to_all | solution.py:86
  148.2 4.2 %all-to-all-start.4 = ((bf16[4,1,256,512]{3,2,1,0:T(8,128)(2,1)}), bf16[4,1,256,512]{3,2,1,0:T(8,128)(2,1)}, u32[]{:S(2)}, u32[]{:S(2)}) async-start(bf16[4,1,256,512]{3,2,1,0:T(8,128)(2,1)} %pad_maximum_fusion), calls=%async_computation.4 | async-start | bytes 2097152 | tf_op jit(solution)/shard_map/all_to_all | solution.py:10
  152.5 2.6 %reshape.246 = bf16[2048,1,256]{2,1,0:T(2,128)(2,1)S(1)} reshape(bf16[4,2,65536]{2,1,0:T(2,128)(2,1)} %copy-done.3) | data formatting | bytes 2097152
  157.8 17.2 %psum.7 = f32[8,64,1]{1,2,0:T(1,128)} all-reduce(f32[8,64,1]{1,2,0:T(1,128)S(1)} %bitcast.128), channel_id=1, replica_groups=mesh['ep'=8,'tp'=4] {'tp'}, use_global_device_ids=true, to_apply=%region_6.7 | all-reduce | flops 512 | bytes 4096 | tf_op jit(solution)/shard_map/psum | solution.py:69
  176.9 4.6 %all-to-all-start.6 = ((f32[8,64,1]{1,2,0:T(1,128)}), f32[8,64,1]{1,2,0:T(1,128)S(1)}, u32[]{:S(2)}, u32[]{:S(2)}) async-start(f32[8,64,1]{1,2,0:T(1,128)} %psum.7), calls=%async_computation.6 | async-start | bytes 8192 | tf_op jit(solution)/shard_map/all_to_all | solution.py:96
  181.6 3.1 %fusion.1 = bf16[8,64,512]{2,1,0:T(8,128)(2,1)} fusion(f32[512,8,64]{0,2,1:T(8,128)S(1)} %convolution_bitcast_fusion.3, bf16[1024,512,1]{1,0,2:T(8,128)(2,1)} %bitcast.38, bf16[8,1,64,1024]{3,2,0,1:T(8,128)(2,1)} %all-gather.11.cloned.1.call-done), kind=kOutput, calls=%fused_computation.12 | convolution fusion | flops 537395200 | bytes 3670016 | tf_op jit(solution)/shard_map/secf,efd->secd/dot_general | solution.py:91
  184.7 2.4 %all-to-all-done.6 = f32[8,64,1]{1,2,0:T(1,128)S(1)} async-done(((f32[8,64,1]{1,2,0:T(1,128)}), f32[8,64,1]{1,2,0:T(1,128)S(1)}, u32[]{:S(2)}, u32[]{:S(2)}) %all-to-all-start.6) | async-done | bytes 2080 | tf_op jit(solution)/shard_map/all_to_all | solution.py:96
  187.0 3.5 %all-to-all-start.5 = ((bf16[8,64,512]{2,1,0:T(8,128)(2,1)}), bf16[8,64,512]{2,1,0:T(8,128)(2,1)S(1)}, u32[]{:S(2)}, u32[]{:S(2)}) async-start(bf16[8,64,512]{2,1,0:T(8,128)(2,1)} %fusion.1), calls=%async_computation.5 | async-start | bytes 1048576 | tf_op jit(solution)/shard_map/all_to_all | solution.py:93
  190.6 3.8 %convolution_bitcast_fusion.2 = f32[1,256,2048]{2,1,0:T(8,128)} fusion(bf16[8,64,2048]{2,1,0:T(8,128)(2,1)} %bitcast.112, bf16[8,1,64,256]{3,2,0,1:T(8,128)(2,1)S(1)} %copy-done.7), kind=kOutput, calls=%fused_computation.8 | convolution fusion | flops 536870912 | bytes 4456448 | tf_op jit(solution)/shard_map/secf,secd->efd/dot_general | solution.py:77
  194.4 2.0 convolution_bitcast_fusion.1
  196.7 2.2 %convolution_bitcast_fusion = f32[1,256,2048]{2,1,0:T(8,128)} fusion(bf16[8,64,2048]{2,1,0:T(8,128)(2,1)S(1)} %bitcast.118, f32[8,64]{1,0:T(8,128)S(1)} %bitcast.125, f32[8,1,64,256]{3,2,0,1:T(8,128)S(1)} %copy-done.11, f32[8,1,64,256]{3,2,0,1:T(8,128)S(1)} %copy-done.13), kind=kOutput, calls=%fused_computation.6 | convolution fusion | flops 537788416 | bytes 5244928 | tf_op jit(solution)/shard_map/secf,secd->efd/dot_general | solution.py:74
  202.8 3.0 %all-to-all-done.5 = bf16[8,64,512]{2,1,0:T(8,128)(2,1)S(1)} async-done(((bf16[8,64,512]{2,1,0:T(8,128)(2,1)}), bf16[8,64,512]{2,1,0:T(8,128)(2,1)S(1)}, u32[]{:S(2)}, u32[]{:S(2)}) %all-to-all-start.5) | async-done | bytes 524320 | tf_op jit(solution)/shard_map/all_to_all | solution.py:93
  (83 shorter events, 24.0 us)
Async XLA Ops:
  7.2 100.2 %copy-start = (bf16[1,256,2048]{2,1,0:T(8,128)(2,1)S(1)}, bf16[1,256,2048]{2,1,0:T(8,128)(2,1)}, u32[]{:S(2)}) copy-start(bf16[1,256,2048]{2,1,0:T(8,128)(2,1)} %param.13) | copy-start | bytes 3145732
  7.2 63.3 %all-gather.7.cloned.1.call-start = ((), (), s32[]{:S(2)}) async-start(), calls=%async_computation.8 | async-start | bytes 2621440 | tf_op jit(solution)/shard_map/all_gather | solution.py:50
  36.3 71.0 %all-gather.5.cloned.1.call-start = ((), (), s32[]{:S(2)}) async-start(), calls=%async_computation.7 | async-start | bytes 2621440 | tf_op jit(solution)/shard_map/all_gather | solution.py:51
  36.4 20.6 %copy-start.14 = (bf16[128,2]{0,1:T(2,128)(2,1)S(1)}, bf16[128,2]{0,1:T(2,128)(2,1)}, u32[]{:S(2)}) copy-start(bf16[128,2]{0,1:T(2,128)(2,1)} %param.10) | copy-start | bytes 1540
  38.4 32.1 %copy-start.8 = (bf16[1,256,2048]{2,1,0:T(8,128)(2,1)S(1)}, bf16[1,256,2048]{2,1,0:T(8,128)(2,1)}, u32[]{:S(2)}) copy-start(bf16[1,256,2048]{2,1,0:T(8,128)(2,1)} %param.12) | copy-start | bytes 3145732
  56.9 118.0 %all-gather.9.cloned.1.call-start = ((), (), s32[]{:S(2)}) async-start(), calls=%async_computation.9 | async-start | bytes 1310720 | tf_op jit(solution)/shard_map/all_gather | solution.py:82
  60.6 13.1 %copy-start.5 = (bf16[1,256,2048]{2,1,0:T(8,128)(2,1)S(1)}, bf16[1,256,2048]{2,1,0:T(8,128)(2,1)}, u32[]{:S(2)}) copy-start(bf16[1,256,2048]{2,1,0:T(8,128)(2,1)} %param.11) | copy-start | bytes 3145732
  70.5 3.3 %copy-start.1 = (bf16[512,2048]{1,0:T(8,128)(2,1)S(1)}, bf16[512,2048]{1,0:T(8,128)(2,1)}, u32[]{:S(2)}) copy-start(bf16[512,2048]{1,0:T(8,128)(2,1)} %all-gather.7.cloned.1.call-done) | copy-start | bytes 6291460
  73.7 33.6 %copy-start.10 = (f32[8,1,64,256]{3,2,0,1:T(8,128)S(1)}, f32[8,1,64,256]{3,2,0,1:T(8,128)}, u32[]{:S(2)}) copy-start(f32[8,1,64,256]{3,2,0,1:T(8,128)} %convolution_bitcast_fusion.5) | copy-start | bytes 1572868
  74.5 36.2 %copy-start.12 = (f32[8,1,64,256]{3,2,0,1:T(8,128)}, f32[8,1,64,256]{3,2,0,1:T(8,128)S(1)}, u32[]{:S(2)}) copy-start(f32[8,1,64,256]{3,2,0,1:T(8,128)S(1)} %convolution_bitcast_fusion.4) | copy-start | bytes 1572868
  127.4 7.7 %copy-start.9 = (bf16[1,256,2048]{2,1,0:T(8,128)(2,1)S(1)}, bf16[1,256,2048]{2,1,0:T(8,128)(2,1)}, u32[]{:S(2)}) copy-start(bf16[1,256,2048]{2,1,0:T(8,128)(2,1)} %param.12) | copy-start | bytes 3145732
  130.9 17.3 %all-to-all-start.3 = ((bf16[4,2,65536]{2,1,0:T(2,128)(2,1)}), bf16[4,2,65536]{2,1,0:T(2,128)(2,1)S(1)}, u32[]{:S(2)}, u32[]{:S(2)}) async-start(bf16[4,2,65536]{2,1,0:T(2,128)(2,1)} %reshape.245), calls=%async_computation.3 | async-start | bytes 2097152 | tf_op jit(solution)/shard_map/all_to_all | solution.py:86
  134.5 47.1 %all-gather.11.cloned.1.call-start = ((), (), s32[]{:S(2)}) async-start(), calls=%async_computation.10 | async-start | bytes 1310720 | tf_op jit(solution)/shard_map/all_gather | solution.py:83
  148.2 4.3 %copy-start.3 = (bf16[4,2,65536]{2,1,0:T(2,128)(2,1)}, bf16[4,2,65536]{2,1,0:T(2,128)(2,1)S(1)}, u32[]{:S(2)}) copy-start(bf16[4,2,65536]{2,1,0:T(2,128)(2,1)S(1)} %all-to-all-done.3) | copy-start | bytes 3145732
  148.2 28.7 %all-to-all-start.4 = ((bf16[4,1,256,512]{3,2,1,0:T(8,128)(2,1)}), bf16[4,1,256,512]{3,2,1,0:T(8,128)(2,1)}, u32[]{:S(2)}, u32[]{:S(2)}) async-start(bf16[4,1,256,512]{3,2,1,0:T(8,128)(2,1)} %pad_maximum_fusion), calls=%async_computation.4 | async-start | bytes 2097152 | tf_op jit(solution)/shard_map/all_to_all | solution.py:10
  176.9 10.1 %all-to-all-start.6 = ((f32[8,64,1]{1,2,0:T(1,128)}), f32[8,64,1]{1,2,0:T(1,128)S(1)}, u32[]{:S(2)}, u32[]{:S(2)}) async-start(f32[8,64,1]{1,2,0:T(1,128)} %psum.7), calls=%async_computation.6 | async-start | bytes 8192 | tf_op jit(solution)/shard_map/all_to_all | solution.py:96
  181.6 9.0 %copy-start.7 = (bf16[8,1,64,256]{3,2,0,1:T(8,128)(2,1)S(1)}, bf16[8,1,64,256]{3,2,0,1:T(8,128)(2,1)}, u32[]{:S(2)}) copy-start(bf16[8,1,64,256]{3,2,0,1:T(8,128)(2,1)} %get-tuple-element.21) | copy-start | bytes 786436
  187.0 18.8 %all-to-all-start.5 = ((bf16[8,64,512]{2,1,0:T(8,128)(2,1)}), bf16[8,64,512]{2,1,0:T(8,128)(2,1)S(1)}, u32[]{:S(2)}, u32[]{:S(2)}) async-start(bf16[8,64,512]{2,1,0:T(8,128)(2,1)} %fusion.1), calls=%async_computation.5 | async-start | bytes 1048576 | tf_op jit(solution)/shard_map/all_to_all | solution.py:93
  190.6 3.8 %copy-start.2 = (bf16[512,2048]{1,0:T(8,128)(2,1)S(1)}, bf16[512,2048]{1,0:T(8,128)(2,1)}, u32[]{:S(2)}) copy-start(bf16[512,2048]{1,0:T(8,128)(2,1)} %all-gather.7.cloned.1.call-done) | copy-start | bytes 6291460
  190.6 3.8 %copy-start.6 = (bf16[8,1,64,256]{3,2,0,1:T(8,128)(2,1)S(1)}, bf16[8,1,64,256]{3,2,0,1:T(8,128)(2,1)}, u32[]{:S(2)}) copy-start(bf16[8,1,64,256]{3,2,0,1:T(8,128)(2,1)} %get-tuple-element.22) | copy-start | bytes 786436
  194.4 2.1 copy-start.4
  194.4 2.1 copy-start.11
  194.4 2.3 %copy-start.13 = (f32[8,1,64,256]{3,2,0,1:T(8,128)S(1)}, f32[8,1,64,256]{3,2,0,1:T(8,128)}, u32[]{:S(2)}) copy-start(f32[8,1,64,256]{3,2,0,1:T(8,128)} %copy-done.12) | copy-start | bytes 1572868
Sparse Core Ops, SparseCore 0:
  36.4 33.9 all-gather.6
  72.3 35.0 all-gather.4
  110.8 26.3 all-gather.8
  138.9 32.5 all-gather.10
